TPU v7x, 32 devices: a whole 2x2x4 slice. The times are simulated.
32 devices in a mesh: ep: 8 (over z, core), tp: 4 (over y, x).
Axes of the slice: x: 2, y: 2, z: 4, core: 2. Of those that a mesh axis runs over, the one named last changes fastest.
Arguments:
- tokens: bfloat16 [4096, 2048], P(('ep', 'tp')), may hold values from -6 to 6
- norm_gain: float32 [2048], replicated, may hold values from 0.1 to 1.9
- expert_ids: int32 [4096, 2], P(('ep', 'tp')), may hold values from 0 to 7, all different within a row; in each aligned block of 128 rows (0 to 127, 128 to 255, ...) at most 64 rows name the same one
- gate_weights: float32 [4096, 2], P(('ep', 'tp')), may hold values from 0.2 to 1.6
- expert_gate: bfloat16 [8, 512, 2048], P('ep', 'tp'), may hold values from -0.125 to 0.125
- expert_up: bfloat16 [8, 512, 2048], P('ep', 'tp'), may hold values from -0.125 to 0.125
- expert_down: bfloat16 [8, 512, 2048], P('ep', 'tp'), may hold values from -0.25 to 0.25
- shared_gate: bfloat16 [512, 2048], P('tp'), may hold values from -0.125 to 0.125
- shared_up: bfloat16 [512, 2048], P('tp'), may hold values from -0.125 to 0.125
- shared_down: bfloat16 [512, 2048], P('tp'), may hold values from -0.25 to 0.25
Outputs:
- mixed: bfloat16 [4096, 2048], P(('ep', 'tp'))
Inputs may be any that keep to these rules, and one draw needn't show every extreme that they name: `expert_ids`: each row names 2 different experts. Within the rows of one device no expert is named by more than 64 rows, and in every draw some expert is named by exactly 64 rows of some device.
All inputs are finite; a program needn't handle non-finite values.
Results may differ from a plain program's by a relative error of at most 0.0068.
Values may be sent and summed in bfloat16 or wider, within the bound.
A program may use at most 64 MiB of HBM per device.

v0:
```python
import jax
import jax.numpy as jnp
from jax import lax
from jax.sharding import PartitionSpec as P

EPS = 1e-06


def for_sending(shard):
    return jax.tree.map(lambda a: a.astype(jnp.bfloat16) if a.dtype == jnp.float32 else a, shard)


def against(rows, weight):
    return lax.dot_general(
        rows, weight, (((1,), (1,)), ((), ())), preferred_element_type=jnp.float32
    )


def hidden_block(rows, gate_rows, up_rows):
    return (jax.nn.silu(against(rows, gate_rows)) * against(rows, up_rows)).astype(jnp.bfloat16)


def apart_mlp(rows, gate, up, down, width, collect_pair, collect_rest):

    def fill_hidden(hidden, pieces, start):
        block = hidden_block(rows, pieces[0], pieces[1])
        return block

    hidden = collect_pair((gate, up), fill_hidden, jnp.zeros((rows.shape[0], width), jnp.bfloat16))

    def add_down(total, piece, start):
        return jnp.dot(hidden, piece, preferred_element_type=jnp.float32)

    empty = jnp.zeros((rows.shape[0], down.shape[1]), jnp.float32)
    return collect_rest(down, add_down, empty)


def body(
    tokens,
    norm_gain,
    expert_ids,
    gate_weights,
    expert_gate,
    expert_up,
    expert_down,
    shared_gate,
    shared_up,
    shared_down,
):
    tok = tokens.astype(jnp.float32)
    normed = (
        tok * lax.rsqrt(jnp.mean(tok * tok, axis=-1, keepdims=True) + EPS) * norm_gain
    ).astype(jnp.bfloat16)
    groups = lax.axis_size("tp")
    count = lax.axis_size("ep")
    tok_rows, chosen = expert_ids.shape
    features = tokens.shape[1]
    capacity = 2 * tok_rows * chosen // count
    labels = jnp.arange(count, dtype=jnp.int32)
    hits = jnp.sum((expert_ids[:, :, None] == labels[None, None, :]).astype(jnp.int32), axis=1)
    before = jnp.cumsum(hits, axis=0) - hits
    slot_of = jnp.take_along_axis(before, expert_ids, axis=1)
    flat_pos = expert_ids * capacity + slot_of
    slots = jnp.arange(count * capacity, dtype=jnp.int32)
    placing = jnp.any(flat_pos[:, :, None] == slots[None, None, :], axis=1).astype(jnp.bfloat16)
    outgoing = lax.dot_general(
        placing, normed, (((0,), (0,)), ((), ())), preferred_element_type=jnp.float32
    )
    outgoing = outgoing.astype(jnp.bfloat16).reshape(count, capacity, features)
    arrived = lax.all_to_all(outgoing, "ep", split_axis=0, concat_axis=0, tiled=True)
    rows = arrived.reshape(count * capacity, features)
    width = expert_gate.shape[1] * groups
    results = apart_mlp(
        rows,
        expert_gate[0],
        expert_up[0],
        expert_down[0],
        width,
        lambda x, fn, init: fn(
            init,
            jax.tree.map(lambda a: lax.all_gather(a, "tp", axis=0, tiled=True), for_sending(x)),
            jnp.int32(0),
        ),
        lambda x, fn, init: fn(init, lax.all_gather(x, "tp", axis=0, tiled=True), jnp.int32(0)),
    )
    results = results.astype(jnp.bfloat16).reshape(count, capacity, features)
    returned = lax.all_to_all(results, "ep", split_axis=0, concat_axis=0, tiled=True).reshape(
        count * capacity, features
    )
    picked = jnp.take(returned, flat_pos.reshape(-1), axis=0).reshape(tok_rows, chosen, features)
    routed = jnp.sum(gate_weights[:, :, None] * picked.astype(jnp.float32), axis=1)
    width = shared_gate.shape[0] * groups
    shared = apart_mlp(
        normed,
        shared_gate,
        shared_up,
        shared_down,
        width,
        lambda x, fn, init: fn(
            init,
            jax.tree.map(lambda a: lax.all_gather(a, "tp", axis=0, tiled=True), for_sending(x)),
            jnp.int32(0),
        ),
        lambda x, fn, init: fn(init, lax.all_gather(x, "tp", axis=0, tiled=True), jnp.int32(0)),
    )
    return (routed + shared).astype(jnp.bfloat16)


def solution(mesh):
    in_specs = (
        P(("ep", "tp"), None),
        P(),
        P(("ep", "tp"), None),
        P(("ep", "tp"), None),
        P("ep", "tp", None),
        P("ep", "tp", None),
        P("ep", "tp", None),
        P("tp", None),
        P("tp", None),
        P("tp", None),
    )
    out_specs = P(("ep", "tp"), None)
    return jax.shard_map(body, mesh=mesh, in_specs=in_specs, out_specs=out_specs, check_vma=False)
```

profile of v0, /device:TPU:0, one launch (start us, length us, event | category | flops | bytes accessed | tf_op | source)
XLA Modules:
  0.0 243.0 jit_solution(15632177701274800440)
XLA Ops:
  6.5 0.0 all-gather.16.cloned.1.call-start
  6.5 0.7 all-gather.16.cloned.1.call-update
  7.3 0.0 all-gather.18.cloned.1.call-start
  7.3 0.7 all-gather.18.cloned.1.call-update
  8.0 0.0 all-gather.20.cloned.1.call-start
  8.1 0.7 all-gather.20.cloned.1.call-update
  8.7 0.0 all-gather.10.cloned.1.call-start
  8.8 0.5 all-gather.10.cloned.1.call-update
  9.3 0.0 copy-done.2
  9.4 0.1 copy.36
  9.5 0.2 reduce_window_sum.11
  9.6 0.1 copy.38
  9.8 0.1 reshape.90
  9.9 0.0 copy-start
  9.9 0.0 copy-start.1
  9.9 1.9 gather_fusion.1
  11.9 0.1 reshape.93
  12.0 0.1 copy.39
  12.1 0.0 copy-done
  12.1 0.2 fusion.13
  12.3 0.1 fusion.19
  12.4 0.0 copy-done.1
  12.5 2.1 convolution_convert_fusion.1
  14.6 6.4 %all-to-all-start = ((bf16[8,64,2048]{2,1,0:T(8,128)(2,1)}), bf16[8,64,2048]{2,1,0:T(8,128)(2,1)S(1)}, u32[]{:S(2)}, u32[]{:S(2)}) async-start(bf16[8,64,2048]{2,1,0:T(8,128)(2,1)} %bitcast.1), calls=%async_computation | async-start | bytes 4194304 | tf_op jit(solution)/shard_map/all_to_all | solution.py:70
  20.9 0.0 all-gather.12.cloned.1.call-start
  21.0 0.5 all-gather.12.cloned.1.call-update
  21.5 25.6 %all-gather.16.cloned.1.call-done = bf16[1,512,2048]{2,1,0:T(8,128)(2,1)} async-done(((bf16[1,128,2048]{2,1,0:T(8,128)(2,1)}), bf16[1,512,2048]{2,1,0:T(8,128)(2,1)}) %all-gather.16.cloned.1.call-update) | async-done | bytes 2097168 | tf_op jit(solution)/shard_map/all_gather | solution.py:81
  47.1 22.9 %all-to-all-done = bf16[8,64,2048]{2,1,0:T(8,128)(2,1)S(1)} async-done(((bf16[8,64,2048]{2,1,0:T(8,128)(2,1)}), bf16[8,64,2048]{2,1,0:T(8,128)(2,1)S(1)}, u32[]{:S(2)}, u32[]{:S(2)}) %all-to-all-start) | async-done | bytes 2097184 | tf_op jit(solution)/shard_map/all_to_all | solution.py:70
  70.0 4.1 %fusion.4 = f32[512,512]{1,0:T(8,128)} fusion(bf16[512,2048]{1,0:T(8,128)(2,1)S(1)} %bitcast.32, bf16[1,512,2048]{2,1,0:T(8,128)(2,1)} %all-gather.16.cloned.1.call-done), kind=kOutput, calls=%fused_computation.9 | convolution fusion | flops 1073741824 | bytes 5242880 | tf_op jit(solution)/shard_map/dot_general | solution.py:14
  74.1 10.0 %all-gather.18.cloned.1.call-done = bf16[1,512,2048]{2,1,0:T(8,128)(2,1)} async-done(((bf16[1,128,2048]{2,1,0:T(8,128)(2,1)}), bf16[1,512,2048]{2,1,0:T(8,128)(2,1)}) %all-gather.18.cloned.1.call-update) | async-done | bytes 2097168 | tf_op jit(solution)/shard_map/all_gather | solution.py:81
  84.2 37.1 %all-gather.20.cloned.1.call-done = bf16[1,512,2048]{2,1,0:T(8,128)(2,1)} async-done(((bf16[1,128,2048]{2,1,0:T(8,128)(2,1)}), bf16[1,512,2048]{2,1,0:T(8,128)(2,1)}) %all-gather.20.cloned.1.call-update) | async-done | bytes 2097168 | tf_op jit(solution)/shard_map/all_gather | solution.py:84
  121.2 6.4 %convolution_convert_fusion = bf16[512,2048]{1,0:T(8,128)(2,1)} fusion(bf16[1,512,2048]{2,1,0:T(8,128)(2,1)} %all-gather.20.cloned.1.call-done, bf16[512,2048]{1,0:T(8,128)(2,1)S(1)} %bitcast.33, bf16[1,512,2048]{2,1,0:T(8,128)(2,1)} %all-gather.18.cloned.1.call-done, f32[512,512]{1,0:T(8,128)} %fusion.4), kind=kOutput, calls=%fused_computation.2 | convolution fusion | flops 2150105088 | bytes 9437184 | tf_op jit(solution)/shard_map/dot_general | solution.py:32
  127.6 4.7 %all-to-all-start.1 = ((bf16[8,64,2048]{2,1,0:T(8,128)(2,1)}), bf16[8,64,2048]{2,1,0:T(8,128)(2,1)S(1)}, u32[]{:S(2)}, u32[]{:S(2)}) async-start(bf16[8,64,2048]{2,1,0:T(8,128)(2,1)} %bitcast.31), calls=%async_computation.1 | async-start | bytes 4194304 | tf_op jit(solution)/shard_map/all_to_all | solution.py:87
  132.4 0.0 all-gather.14.cloned.1.call-start
  132.4 0.5 all-gather.14.cloned.1.call-update
  132.9 0.1 copy.41
  133.0 0.1 reshape.81
  133.2 0.1 copy.40
  133.3 0.1 copy.35
  133.5 24.7 %all-gather.10.cloned.1.call-done = bf16[512,2048]{1,0:T(8,128)(2,1)} async-done(((bf16[128,2048]{1,0:T(8,128)(2,1)}), bf16[512,2048]{1,0:T(8,128)(2,1)}) %all-gather.10.cloned.1.call-update) | async-done | bytes 2097168 | tf_op jit(solution)/shard_map/all_gather | solution.py:101
  158.1 2.4 fusion.31
  160.6 20.8 %all-to-all-done.1 = bf16[8,64,2048]{2,1,0:T(8,128)(2,1)S(1)} async-done(((bf16[8,64,2048]{2,1,0:T(8,128)(2,1)}), bf16[8,64,2048]{2,1,0:T(8,128)(2,1)S(1)}, u32[]{:S(2)}, u32[]{:S(2)}) %all-to-all-start.1) | async-done | bytes 2097184 | tf_op jit(solution)/shard_map/all_to_all | solution.py:87
  181.4 2.3 gather_fusion
  183.7 1.7 gather.12
  185.5 4.1 %multiply_reduce_fusion = f32[128,2048]{1,0:T(8,128)S(1)} fusion(bf16[128,2,2048]{2,1,0:T(2,128)(2,1)S(1)} %gather.12, pred[128,2]{1,0:T(8,128)(4,1)S(1)} %copy.40, f32[128,2]{1,0:T(8,128)S(1)} %copy.35), kind=kLoop, calls=%fused_computation.11 | loop fusion | flops 1835008 | bytes 2098432 | tf_op jit(solution)/shard_map/reduce_sum | solution.py:91
  189.6 5.5 %all-gather.12.cloned.1.call-done = bf16[512,2048]{1,0:T(8,128)(2,1)} async-done(((bf16[128,2048]{1,0:T(8,128)(2,1)}), bf16[512,2048]{1,0:T(8,128)(2,1)}) %all-gather.12.cloned.1.call-update) | async-done | bytes 2097168 | tf_op jit(solution)/shard_map/all_gather | solution.py:101
  195.0 36.9 %all-gather.14.cloned.1.call-done = bf16[512,2048]{1,0:T(8,128)(2,1)} async-done(((bf16[128,2048]{1,0:T(8,128)(2,1)}), bf16[512,2048]{1,0:T(8,128)(2,1)}) %all-gather.14.cloned.1.call-update) | async-done | bytes 2097168 | tf_op jit(solution)/shard_map/all_gather | solution.py:104
  231.9 4.3 %fusion = bf16[128,2048]{1,0:T(8,128)(2,1)} fusion(f32[128,2048]{1,0:T(8,128)S(1)} %multiply_reduce_fusion, bf16[512,2048]{1,0:T(8,128)(2,1)} %all-gather.14.cloned.1.call-done, bf16[512,2048]{1,0:T(8,128)(2,1)} %all-gather.12.cloned.1.call-done, f32[128,512]{1,0:T(8,128)S(1)} %fusion.31, bf16[128,2048]{1,0:T(8,128)(2,1)S(1)} %copy-done, ...), kind=kOutput, calls=%fused_computation.5 | convolution fusion | flops 538836992 | bytes 6562304 | tf_op jit(solution)/shard_map/dot_general | solution.py:32
  (10 shorter events, 0.1 us)
Async XLA Ops:
  6.5 2.8 %copy-start.2 = (s32[128,2]{0,1:T(2,128)S(1)}, s32[128,2]{0,1:T(2,128)}, u32[]{:S(2)}) copy-start(s32[128,2]{0,1:T(2,128)} %param.12) | copy-start | bytes 3076
  6.5 40.6 %all-gather.16.cloned.1.call-start = ((), (), s32[]{:S(2)}) async-start(), calls=%async_computation.5 | async-start | bytes 2621440 | tf_op jit(solution)/shard_map/all_gather | solution.py:81
  7.3 76.9 %all-gather.18.cloned.1.call-start = ((), (), s32[]{:S(2)}) async-start(), calls=%async_computation.6 | async-start | bytes 2621440 | tf_op jit(solution)/shard_map/all_gather | solution.py:81
  8.0 113.2 %all-gather.20.cloned.1.call-start = ((), (), s32[]{:S(2)}) async-start(), calls=%async_computation.7 | async-start | bytes 2621440 | tf_op jit(solution)/shard_map/all_gather | solution.py:84
  8.7 149.4 %all-gather.10.cloned.1.call-start = ((), (), s32[]{:S(2)}) async-start(), calls=%async_computation.2 | async-start | bytes 2621440 | tf_op jit(solution)/shard_map/all_gather | solution.py:101
  9.9 2.2 copy-start
  9.9 2.5 %copy-start.1 = (f32[2048]{0:T(1024)S(1)}, f32[2048]{0:T(1024)}, u32[]{:S(2)}) copy-start(f32[2048]{0:T(1024)} %param.11) | copy-start | bytes 24580
  14.6 55.4 %all-to-all-start = ((bf16[8,64,2048]{2,1,0:T(8,128)(2,1)}), bf16[8,64,2048]{2,1,0:T(8,128)(2,1)S(1)}, u32[]{:S(2)}, u32[]{:S(2)}) async-start(bf16[8,64,2048]{2,1,0:T(8,128)(2,1)} %bitcast.1), calls=%async_computation | async-start | bytes 4194304 | tf_op jit(solution)/shard_map/all_to_all | solution.py:70
  20.9 174.1 %all-gather.12.cloned.1.call-start = ((), (), s32[]{:S(2)}) async-start(), calls=%async_computation.3 | async-start | bytes 2621440 | tf_op jit(solution)/shard_map/all_gather | solution.py:101
  127.6 5.7 %copy-start.3 = (f32[128,2]{0,1:T(2,128)S(1)}, f32[128,2]{0,1:T(2,128)}, u32[]{:S(2)}) copy-start(f32[128,2]{0,1:T(2,128)} %param.13) | copy-start | bytes 3076
  127.6 53.8 %all-to-all-start.1 = ((bf16[8,64,2048]{2,1,0:T(8,128)(2,1)}), bf16[8,64,2048]{2,1,0:T(8,128)(2,1)S(1)}, u32[]{:S(2)}, u32[]{:S(2)}) async-start(bf16[8,64,2048]{2,1,0:T(8,128)(2,1)} %bitcast.31), calls=%async_computation.1 | async-start | bytes 4194304 | tf_op jit(solution)/shard_map/all_to_all | solution.py:87
  132.4 99.6 %all-gather.14.cloned.1.call-start = ((), (), s32[]{:S(2)}) async-start(), calls=%async_computation.4 | async-start | bytes 2621440 | tf_op jit(solution)/shard_map/all_gather | solution.py:104
Sparse Core Ops, SparseCore 0:
  9.2 37.8 all-gather.15
  49.0 35.1 all-gather.17
  86.0 35.1 all-gather.19
  122.9 35.1 all-gather.9
  159.8 35.1 all-gather.11
  196.7 35.1 all-gather.13
where the time goes:
time: 243 us
  waiting for transfers between devices  187 us (77%)
  matrix products  19.4 us (8%)
  between operations  13.6 us (6%)
  starting transfers between devices  11.3 us (5%)
  local copies, waits for them, and re-layouts  7.09 us (3%)
  other arithmetic  4.61 us (2%)
    all_gather x2, waiting for transfers between devices, body(): lax.all_gather(x, 'tp', axis=0, tiled=True)  74 us
    all_gather x4, waiting for transfers between devices, body(): lax.all_gather(a, 'tp', axis=0, tiled=True)  65.8 us
    all_to_all x1, waiting for transfers between devices, body(): lax.all_to_all(outgoing, 'ep', split_axis=0, concat_axis=0, tiled=True)  22.9 us
    all_to_all x1, waiting for transfers between devices, body(): lax.all_to_all(results, 'ep', split_axis=0, concat_axis=0, tiled=True)  20.8 us
    dot_general x2, matrix products, add_down(): return jnp.dot(hidden, piece, preferred_element_type=jnp.float32)  10.7 us
    dot_general x2, matrix products, against(): lax.dot_general(rows, weight, (((1,), (1,)), ((), ())), preferred_element...  6.57 us
    all_to_all x1, starting transfers between devices, body(): lax.all_to_all(outgoing, 'ep', split_axis=0, concat_axis=0, tiled=True)  6.35 us
  transfers between devices with their start and end apart: 8, of which 8 were waited for; matrix products, arithmetic and copies ran while one was open for 11% of the time, Pallas kernels for 0%

commit v1 on v0

v1 whole, which is shorter than its diff:
```python
import functools
import math

import jax
import jax.numpy as jnp
from jax import lax
from jax.experimental import pallas as pl
from jax.experimental.pallas import tpu as pltpu
from jax.sharding import PartitionSpec as P

EPS = 1e-06
MESH = pl.DeviceIdType.MESH
NT = (((1,), (1,)), ((), ()))
F32 = jnp.float32
BF16 = jnp.bfloat16


def remote(src, dst, send, recv, where):
    return pltpu.make_async_remote_copy(
        src_ref=src, dst_ref=dst, send_sem=send, recv_sem=recv, device_id=where, device_id_type=MESH
    )


def kernel(
    ep, tp, xs, ys, cap,
    tok_ref, gain_ref, ids_ref, gw_ref, eg, eu, ed, sg, su, sd, out_ref,
    wts, swts, normed, mix, outgoing, arrived, hidden, results, returned,
    s1, r1, s2, r2, s3, r3, sa, ra, sb, rb,
):
    e = lax.axis_index("ep")
    t = lax.axis_index("tp")
    y, x = t // xs, t % xs
    core = e % 2
    partner = e + 1 - 2 * core
    d_model = tok_ref.shape[1]
    rows = tok_ref.shape[0]
    half = d_model // 2
    own_rows = eg.shape[0]
    srows = sg.shape[0] // 2
    slots = ep * cap

    def at(dy, dx):
        return lax.rem(y + dy, ys) * xs + lax.rem(x + dx, xs)

    row_peers = [at(0, i) for i in range(1, xs)]
    col_peers = [at(i, 0) for i in range(1, ys)]
    diagonal = [at(i, j) for i in range(1, ys) for j in range(1, xs)]
    ep_peers = [lax.rem(e + i, ep) for i in range(1, ep)]

    barrier = pltpu.get_barrier_semaphore()
    for p in row_peers + col_peers:
        pl.semaphore_signal(barrier, inc=1, device_id={"tp": p}, device_id_type=MESH)
    for p in ep_peers:
        pl.semaphore_signal(barrier, inc=1, device_id={"ep": p}, device_id_type=MESH)
    pl.semaphore_wait(barrier, len(row_peers) + len(col_peers) + len(ep_peers))

    ins = (eg, eu, ed, sg, su, sd)
    sends = []

    def block(a, owner):
        return wts.at[a, owner] if a < 3 else swts.at[a - 3, core, owner]

    def part(a, owner, h):
        cols = pl.ds(h * half, half)
        return wts.at[a, owner, :, cols] if a < 3 else swts.at[a - 3, core, owner, :, cols]

    def own(a):
        return ins[a] if a < 3 else ins[a].at[pl.ds(pl.multiple_of(core * srows, srows), srows)]

    def first(a):
        for j, p in enumerate(row_peers + col_peers):
            c = remote(own(a), block(a, t), s1.at[a, j], r1.at[a, t], {"tp": p})
            c.start()
            sends.append(c)

    def first_done(a):
        for q in row_peers + col_peers:
            remote(block(a, q), block(a, q), s1.at[a, 0], r1.at[a, q], {"tp": q}).wait_recv()

    def second(a):
        for h, (owners, peers) in enumerate(((col_peers, row_peers), (row_peers, col_peers))):
            for i, q in enumerate(owners):
                for j, p in enumerate(peers):
                    c = remote(part(a, q, h), part(a, q, h), s2.at[a, h, i, j], r2.at[a, h, q], {"tp": p})
                    c.start()
                    sends.append(c)

    def second_done(a):
        for q in diagonal:
            for h in range(2):
                remote(part(a, q, h), part(a, q, h), s2.at[a, h, 0, 0], r2.at[a, h, q], {"tp": q}).wait_recv()

    first(0)
    first(1)

    tok = tok_ref[...].astype(F32)
    nrm = tok * lax.rsqrt(jnp.mean(tok * tok, axis=-1, keepdims=True) + EPS) * gain_ref[...]
    normed[...] = nrm.astype(BF16)
    ids = ids_ref[...]
    chosen = ids.shape[1]
    labels = lax.broadcasted_iota(jnp.int32, (rows, ep), 1)
    one_hot = [(ids[:, k : k + 1] == labels).astype(F32) for k in range(chosen)]
    hits = sum(one_hot[1:], one_hot[0])
    lower = (
        lax.broadcasted_iota(jnp.int32, (rows, rows), 1) < lax.broadcasted_iota(jnp.int32, (rows, rows), 0)
    ).astype(F32).astype(BF16)
    before = jnp.dot(lower, hits.astype(BF16), preferred_element_type=F32)
    slot_ids = lax.broadcasted_iota(jnp.int32, (rows, slots), 1).astype(F32)
    weights = jnp.zeros((rows, slots), F32)
    placing = jnp.zeros((rows, slots), F32)
    for k in range(chosen):
        place = ids[:, k : k + 1].astype(F32) * cap + jnp.sum(before * one_hot[k], axis=1, keepdims=True)
        hit = (place == slot_ids).astype(F32)
        placing = placing + hit
        weights = weights + gw_ref[:, k : k + 1] * hit
    high = weights.astype(BF16)
    mix[0] = high
    mix[1] = (weights - high.astype(F32)).astype(BF16)
    spread = placing.T.astype(BF16)
    for n in range(4):
        cols = slice(n * (d_model // 4), (n + 1) * (d_model // 4))
        o = jnp.dot(spread, normed[:, cols], preferred_element_type=F32).astype(BF16)
        outgoing[:, :, cols] = o.reshape(ep, cap, d_model // 4)

    for j, p in enumerate(ep_peers):
        c = remote(outgoing.at[p], arrived.at[e], sa.at[j], ra.at[e], {"ep": p})
        c.start()
        sends.append(c)
    arrived[e] = outgoing[e]
    for a in range(3):
        wts[a, t] = ins[a][...]
        swts[a, core, t] = ins[a + 3][pl.ds(pl.multiple_of(core * srows, srows), srows), :]

    first_done(0)
    second(0)
    first(2)
    first_done(1)
    second(1)
    first_done(2)
    second(2)
    first(3)
    first(4)

    for p in ep_peers:
        remote(arrived.at[p], arrived.at[p], sa.at[0], ra.at[p], {"ep": p}).wait_recv()
    second_done(0)
    second_done(1)
    per = max(1, min(tp, 256 // own_rows))
    chunks = tp // per
    width = per * own_rows
    for c in range(chunks):
        held = arrived[...].reshape(slots, d_model)
        gate = lax.dot_general(held, wts[0, c * per : (c + 1) * per].reshape(width, d_model), NT, preferred_element_type=F32)
        up = lax.dot_general(held, wts[1, c * per : (c + 1) * per].reshape(width, d_model), NT, preferred_element_type=F32)
        hidden[:, c * width : (c + 1) * width] = (gate * (1.0 / (1.0 + jnp.exp(-gate))) * up).astype(BF16)
    second_done(2)
    for n in range(4):
        cols = slice(n * (d_model // 4), (n + 1) * (d_model // 4))
        down = wts[2, :, :, cols].reshape(tp * own_rows, d_model // 4)
        o = jnp.dot(hidden[...], down, preferred_element_type=F32).astype(BF16)
        results[:, :, cols] = o.reshape(ep, cap, d_model // 4)
    for j, p in enumerate(ep_peers):
        c = remote(results.at[p], returned.at[e], sb.at[j], rb.at[e], {"ep": p})
        c.start()
        sends.append(c)
    returned[e] = results[e]

    first_done(3)
    second(3)
    first(5)
    first_done(4)
    second(4)
    first_done(5)
    second(5)

    def swap(a):
        return remote(swts.at[a, core], swts.at[a, core], s3.at[a], r3.at[a], {"ep": partner})

    for a in range(3):
        second_done(a + 3)
        c = swap(a)
        c.start()
        sends.append(c)
    for a in range(3):
        other = swts.at[a, 1 - core]
        remote(other, other, s3.at[a], r3.at[a], {"ep": partner}).wait_recv()
    sall = swts.shape[1] * tp * srows
    gate = lax.dot_general(normed[...], swts[0].reshape(sall, d_model), NT, preferred_element_type=F32)
    up = lax.dot_general(normed[...], swts[1].reshape(sall, d_model), NT, preferred_element_type=F32)
    shared_hidden = (gate * (1.0 / (1.0 + jnp.exp(-gate))) * up).astype(BF16)

    for p in ep_peers:
        remote(returned.at[p], returned.at[p], sb.at[0], rb.at[p], {"ep": p}).wait_recv()
    for n in range(4):
        cols = slice(n * (d_model // 4), (n + 1) * (d_model // 4))
        sdown = swts[2, :, :, :, cols].reshape(sall, d_model // 4)
        back = returned[:, :, cols].reshape(slots, d_model // 4)
        total = jnp.dot(mix[0], back, preferred_element_type=F32)
        total = total + jnp.dot(mix[1], back, preferred_element_type=F32)
        total = total + jnp.dot(shared_hidden, sdown, preferred_element_type=F32)
        out_ref[:, cols] = total.astype(BF16)
    for c in sends:
        c.wait_send()


def body(ep, tp, tokens, norm_gain, expert_ids, gate_weights, eg, eu, ed, sg, su, sd):
    rows, d_model = tokens.shape
    cap = 2 * rows * expert_ids.shape[1] // ep
    side = math.isqrt(tp)
    xs = side if side * side == tp else tp
    ys = tp // xs
    own_rows = eg.shape[1]
    srows = sg.shape[0] // 2
    near = xs + ys - 2
    far = max(xs, ys)
    dma = pltpu.SemaphoreType.DMA
    vm = pl.BlockSpec(memory_space=pltpu.VMEM)
    return pl.pallas_call(
        functools.partial(kernel, ep, tp, xs, ys, cap),
        out_shape=jax.ShapeDtypeStruct((rows, d_model), BF16),
        in_specs=[vm] * 10,
        out_specs=vm,
        scratch_shapes=[
            pltpu.VMEM((3, tp, own_rows, d_model), BF16),
            pltpu.VMEM((3, 2, tp, srows, d_model), BF16),
            pltpu.VMEM((rows, d_model), BF16),
            pltpu.VMEM((2, rows, ep * cap), BF16),
            pltpu.VMEM((ep, cap, d_model), BF16),
            pltpu.VMEM((ep, cap, d_model), BF16),
            pltpu.VMEM((ep * cap, tp * own_rows), BF16),
            pltpu.VMEM((ep, cap, d_model), BF16),
            pltpu.VMEM((ep, cap, d_model), BF16),
            dma((6, near)),
            dma((6, tp)),
            dma((6, 2, far, far)),
            dma((6, 2, tp)),
            dma((3,)),
            dma((3,)),
            dma((ep,)),
            dma((ep,)),
            dma((ep,)),
            dma((ep,)),
        ],
        compiler_params=pltpu.CompilerParams(
            collective_id=0, has_side_effects=True, vmem_limit_bytes=62 * 1024 * 1024
        ),
        name="moe",
    )(tokens, norm_gain.reshape(1, d_model), expert_ids, gate_weights, eg[0], eu[0], ed[0], sg, su, sd)


def solution(mesh):
    in_specs = (
        P(("ep", "tp"), None),
        P(),
        P(("ep", "tp"), None),
        P(("ep", "tp"), None),
        P("ep", "tp", None),
        P("ep", "tp", None),
        P("ep", "tp", None),
        P("tp", None),
        P("tp", None),
        P("tp", None),
    )
    out_specs = P(("ep", "tp"), None)
    return jax.shard_map(
        functools.partial(body, mesh.shape["ep"], mesh.shape["tp"]),
        mesh=mesh, in_specs=in_specs, out_specs=out_specs, check_vma=False,
    )
```

time: 243 us -> 112 us (0.46)
  the two profiles are of different devices: /device:TPU:0 before, /device:TPU:9 now
where the time goes in v1:
time: 112 us
  Pallas kernels  108 us (96%)
  local copies, waits for them, and re-layouts  4.03 us (4%)
    pallas_call x1, Pallas kernels, body(): pl.pallas_call(functools.partial(kernel, ep, tp, xs, ys, cap), out_shape=...  108 us
    unnamed x7, local copies, waits for them, and re-layouts  4.03 us

profile of v1, /device:TPU:9, one launch (start us, length us, event | category | flops | bytes accessed | tf_op | source)
XLA Modules:
  0.0 112.1 jit_solution(1448125561019563905)
XLA Ops:
  0.0 0.0 copy-start
  0.0 0.7 copy-done
  0.7 0.0 copy-start.1
  0.7 0.7 copy.11.ids_ref
  1.4 0.0 copy-done.1
  1.4 0.7 copy.12.gw_ref
  2.2 108.1 %moe.1 = bf16[128,2048]{1,0:T(8,128)(2,1)} custom-call(bf16[128,2048]{1,0:T(8,128)(2,1)} %tok_ref.1, f32[1,2048]{1,0:T(1,128)} %bitcast.7, s32[128,2]{1,0:T(8,128)} %copy.11.ids_ref, f32[128,2]{1,0:T(8,128)} %copy.12.gw_ref, bf16[128,2048]{1,0:T(8,128)(2,1)} %bitcast.4, bf16[128,2048]{1,0:T(8,128)(2,1)} %bitcast.5, bf16[128,2048]{1,0:T(8,128)(2,1)} %bitcast.6, ...), custom_call_target="tpu_custom_call" | custom-call | tf_op jit(solution)/shard_map/moe/pallas_call | solution.py:218
  110.2 1.9 %copy.14 = bf16[128,2048]{1,0:T(8,128)(2,1)} copy(bf16[128,2048]{1,0:T(8,128)(2,1)} %moe.1) | data formatting | bytes 1048576
Async XLA Ops:
  0.0 0.7 copy-start
  0.7 0.7 copy-start.1

commit v2 on v1

v2 whole, which is shorter than its diff:
```python
import functools
import math

import jax
import jax.numpy as jnp
from jax import lax
from jax.experimental import pallas as pl
from jax.experimental.pallas import tpu as pltpu
from jax.sharding import PartitionSpec as P

EPS = 1e-06
MESH = pl.DeviceIdType.MESH
NT = (((1,), (1,)), ((), ()))
F32 = jnp.float32
BF16 = jnp.bfloat16
CHUNKS = 4


def remote(src, dst, send, recv, where):
    return pltpu.make_async_remote_copy(
        src_ref=src, dst_ref=dst, send_sem=send, recv_sem=recv, device_id=where, device_id_type=MESH
    )


def kernel(
    ep, tp, xs, ys, cap,
    tok_ref, gain_ref, ids_ref, gw_ref, eg, eu, ed, sg, su, sd, out_ref,
    wts, swts, normed, mix, spread, pick, tokens, arrived, hidden, results, returned,
    s1, r1, s2, r2, s3, r3, sp, rp, st, rt, sd2, rd2, sb, rb,
):
    e = lax.axis_index("ep")
    t = lax.axis_index("tp")
    y, x = t // xs, t % xs
    z, core = e // 2, e % 2
    nz = ep // 2
    partner = e + 1 - 2 * core
    rows, d_model = tok_ref.shape
    own_rows = eg.shape[0]
    srows = sg.shape[0] // 2
    slots = ep * cap
    piece = d_model // CHUNKS
    last = 2 + CHUNKS

    def at(dy, dx):
        return lax.rem(y + dy, ys) * xs + lax.rem(x + dx, xs)

    row_peers = [at(0, i) for i in range(1, xs)]
    col_peers = [at(i, 0) for i in range(1, ys)]
    diagonal = [at(i, j) for i in range(1, ys) for j in range(1, xs)]
    ep_peers = [lax.rem(e + i, ep) for i in range(1, ep)]

    barrier = pltpu.get_barrier_semaphore()
    for p in row_peers + col_peers:
        pl.semaphore_signal(barrier, inc=1, device_id={"tp": p}, device_id_type=MESH)
    for p in ep_peers:
        pl.semaphore_signal(barrier, inc=1, device_id={"ep": p}, device_id_type=MESH)
    pl.semaphore_wait(barrier, len(row_peers) + len(col_peers) + len(ep_peers))

    sends = []
    mine = pl.ds(pl.multiple_of(core * srows, srows), srows)

    def columns(a):
        return ((a - 2) * piece, piece) if 2 <= a < last else (0, d_model)

    def view(a, owner, start, size):
        cols = pl.ds(start, size)
        if a < last:
            return wts.at[min(a, 2), owner, :, cols]
        return swts.at[a - last, core, owner, :, cols]

    def block(a, owner):
        return view(a, owner, *columns(a))

    def part(a, owner, h):
        start, size = columns(a)
        return view(a, owner, start + h * (size // 2), size // 2)

    def own(a):
        if a < last:
            start, size = columns(a)
            return (eg, eu, ed)[min(a, 2)].at[:, pl.ds(start, size)]
        return (sg, su, sd)[a - last].at[mine]

    def first(a):
        for j, p in enumerate(row_peers + col_peers):
            c = remote(own(a), block(a, t), s1.at[a, j], r1.at[a, t], {"tp": p})
            c.start()
            sends.append(c)

    def first_done(a):
        for q in row_peers + col_peers:
            remote(block(a, q), block(a, q), s1.at[a, 0], r1.at[a, q], {"tp": q}).wait_recv()

    def second(a):
        for h, (owners, peers) in enumerate(((col_peers, row_peers), (row_peers, col_peers))):
            for i, q in enumerate(owners):
                for j, p in enumerate(peers):
                    c = remote(part(a, q, h), part(a, q, h), s2.at[a, h, i, j], r2.at[a, h, q], {"tp": p})
                    c.start()
                    sends.append(c)

    def second_done(a):
        for q in diagonal:
            for h in range(2):
                remote(part(a, q, h), part(a, q, h), s2.at[a, h, 0, 0], r2.at[a, h, q], {"tp": q}).wait_recv()

    def hop(src, sign, source):
        slot = 2 * src + core
        d = 0 if sign > 0 else 1
        return remote(source, tokens.at[slot], st.at[d, src], rt.at[src], {"ep": e + 2 * sign})

    def over(src, source):
        slot = 2 * src + core
        return remote(source, tokens.at[slot], sd2.at[src], rd2.at[src], {"ep": partner})

    def from_partner(src):
        slot = 2 * src + 1 - core
        return remote(tokens.at[slot], tokens.at[slot], sd2.at[src], rd2.at[src], {"ep": partner})

    def pack(src_ep, source):
        raw = jnp.dot(pick[src_ep], source[...], preferred_element_type=F32)
        scale = lax.rsqrt(jnp.mean(raw * raw, axis=-1, keepdims=True) + EPS)
        arrived[src_ep] = (raw * scale * gain_ref[...]).astype(BF16)

    def pick_done(src_ep):
        remote(pick.at[src_ep], pick.at[src_ep], sp.at[0], rp.at[src_ep], {"ep": partner}).wait_recv()

    first(0)

    @pl.when(z + 1 < nz)
    def _():
        hop(z, 1, tok_ref).start()

    @pl.when(z > 0)
    def _():
        hop(z, -1, tok_ref).start()

    over(z, tok_ref).start()
    first(1)

    ids = ids_ref[...]
    chosen = ids.shape[1]
    labels = lax.broadcasted_iota(jnp.int32, (rows, ep), 1)
    one_hot = [(ids[:, k : k + 1] == labels).astype(F32) for k in range(chosen)]
    hits = sum(one_hot[1:], one_hot[0])
    lower = (
        lax.broadcasted_iota(jnp.int32, (rows, rows), 1) < lax.broadcasted_iota(jnp.int32, (rows, rows), 0)
    ).astype(F32).astype(BF16)
    before = jnp.dot(lower, hits.astype(BF16), preferred_element_type=F32)
    slot_ids = lax.broadcasted_iota(jnp.int32, (rows, slots), 1).astype(F32)
    weights = jnp.zeros((rows, slots), F32)
    placing = jnp.zeros((rows, slots), F32)
    for k in range(chosen):
        place = ids[:, k : k + 1].astype(F32) * cap + jnp.sum(before * one_hot[k], axis=1, keepdims=True)
        hit = (place == slot_ids).astype(F32)
        placing = placing + hit
        weights = weights + gw_ref[:, k : k + 1] * hit
    spread[...] = placing.T.astype(BF16).reshape(ep, cap, rows)
    high = weights.astype(BF16)
    mix[0] = high
    mix[1] = (weights - high.astype(F32)).astype(BF16)
    for j, p in enumerate(ep_peers):
        c = remote(spread.at[p], pick.at[e], sp.at[j], rp.at[e], {"ep": p})
        c.start()
        sends.append(c)
    pick[e] = spread[e]
    tok = tok_ref[...].astype(F32)
    nrm = tok * lax.rsqrt(jnp.mean(tok * tok, axis=-1, keepdims=True) + EPS) * gain_ref[...]
    normed[...] = nrm.astype(BF16)
    for a, ref in enumerate((eg, eu, ed)):
        wts[a, t] = ref[...]
    for a, ref in enumerate((sg, su, sd)):
        swts[a, core, t] = ref[mine, :]
    pack(e, tok_ref)
    for p in ep_peers:
        pick_done(p)
    from_partner(z).wait_recv()
    pack(partner, tokens.at[partner])

    first_done(0)
    second(0)

    def packs(step):
        for sign in (1, -1):
            src = z - sign * (step + 1)
            there = (src >= 0) if sign > 0 else (src < nz)

            @pl.when(there)
            def _():
                pack(2 * src + core, tokens.at[2 * src + core])
                from_partner(src).wait_recv()
                pack(2 * src + 1 - core, tokens.at[2 * src + 1 - core])

    for step in range(nz - 1):
        for sign in (1, -1):
            src = z - sign * (step + 1)
            there = (src >= 0) if sign > 0 else (src < nz)
            on = (z + 1 < nz) if sign > 0 else (z > 0)

            @pl.when(there)
            def _():
                here = tokens.at[2 * src + core]
                hop(src, sign, here).wait_recv()

                @pl.when(on)
                def _():
                    hop(src, sign, here).start()

                over(src, here).start()

        if step == 0:
            packs(0)
            first_done(1)
            second(1)
            first(2)
            first(3)
        else:
            packs(step)
    if nz == 1:
        first_done(1)
        second(1)
        first(2)
        first(3)

    second_done(0)
    second_done(1)
    per = max(1, min(tp, 256 // own_rows))
    width = per * own_rows
    for c in range(tp // per):
        held = arrived[...].reshape(slots, d_model)
        gate = lax.dot_general(held, wts[0, c * per : (c + 1) * per].reshape(width, d_model), NT, preferred_element_type=F32)
        up = lax.dot_general(held, wts[1, c * per : (c + 1) * per].reshape(width, d_model), NT, preferred_element_type=F32)
        hidden[:, c * width : (c + 1) * width] = (gate * (1.0 / (1.0 + jnp.exp(-gate))) * up).astype(BF16)

    def back(n, p, j):
        cols = pl.ds(n * piece, piece)
        return remote(results.at[p, :, cols], returned.at[e, :, cols], sb.at[n, j], rb.at[n, e], {"ep": p})

    total = last + 3
    for n in range(CHUNKS):
        a = n + 2
        if n == 0:
            first_done(a)
            second(a)
            first(a + 2)
        first_done(a + 1)
        second(a + 1)
        if a + 3 < total:
            first(a + 3)
        second_done(a)
        cols = slice(n * piece, (n + 1) * piece)
        down = wts[2, :, :, cols].reshape(tp * own_rows, piece)
        o = jnp.dot(hidden[...], down, preferred_element_type=F32).astype(BF16)
        results[:, :, cols] = o.reshape(ep, cap, piece)
        for j, p in enumerate(ep_peers):
            c = back(n, p, j)
            c.start()
            sends.append(c)
        returned[e, :, cols] = results[e, :, cols]

    def swap(a):
        return remote(swts.at[a, core], swts.at[a, core], s3.at[a], r3.at[a], {"ep": partner})

    for a in range(3):
        if a > 0:
            first_done(last + a)
            second(last + a)
        second_done(last + a)
        c = swap(a)
        c.start()
        sends.append(c)
    for a in range(3):
        other = swts.at[a, 1 - core]
        remote(other, other, s3.at[a], r3.at[a], {"ep": partner}).wait_recv()
    sall = 2 * tp * srows
    gate = lax.dot_general(normed[...], swts[0].reshape(sall, d_model), NT, preferred_element_type=F32)
    up = lax.dot_general(normed[...], swts[1].reshape(sall, d_model), NT, preferred_element_type=F32)
    shared_hidden = (gate * (1.0 / (1.0 + jnp.exp(-gate))) * up).astype(BF16)

    for n in range(CHUNKS):
        cols = slice(n * piece, (n + 1) * piece)
        sdown = swts[2, :, :, :, cols].reshape(sall, piece)
        sum_shared = jnp.dot(shared_hidden, sdown, preferred_element_type=F32)
        for p in ep_peers:
            c = returned.at[p, :, pl.ds(n * piece, piece)]
            remote(c, c, sb.at[0, 0], rb.at[n, p], {"ep": p}).wait_recv()
        given = returned[:, :, cols].reshape(slots, piece)
        routed = jnp.dot(mix[0], given, preferred_element_type=F32)
        routed = routed + jnp.dot(mix[1], given, preferred_element_type=F32)
        out_ref[:, cols] = (routed + sum_shared).astype(BF16)
    for c in sends:
        c.wait_send()

    over(z, tok_ref).wait_send()

    @pl.when(z + 1 < nz)
    def _():
        hop(z, 1, tok_ref).wait_send()

    @pl.when(z > 0)
    def _():
        hop(z, -1, tok_ref).wait_send()

    for step in range(nz - 1):
        for sign in (1, -1):
            src = z - sign * (step + 1)
            there = (src >= 0) if sign > 0 else (src < nz)
            on = (z + 1 < nz) if sign > 0 else (z > 0)

            @pl.when(there)
            def _():
                here = tokens.at[2 * src + core]
                over(src, here).wait_send()

                @pl.when(on)
                def _():
                    hop(src, sign, here).wait_send()


def body(ep, tp, tokens, norm_gain, expert_ids, gate_weights, eg, eu, ed, sg, su, sd):
    rows, d_model = tokens.shape
    cap = 2 * rows * expert_ids.shape[1] // ep
    side = math.isqrt(tp)
    xs = side if side * side == tp else tp
    ys = tp // xs
    own_rows = eg.shape[1]
    srows = sg.shape[0] // 2
    near = xs + ys - 2
    far = max(xs, ys)
    moves = 2 + CHUNKS + 3
    dma = pltpu.SemaphoreType.DMA
    vm = pl.BlockSpec(memory_space=pltpu.VMEM)
    return pl.pallas_call(
        functools.partial(kernel, ep, tp, xs, ys, cap),
        out_shape=jax.ShapeDtypeStruct((rows, d_model), BF16),
        in_specs=[vm] * 10,
        out_specs=vm,
        scratch_shapes=[
            pltpu.VMEM((3, tp, own_rows, d_model), BF16),
            pltpu.VMEM((3, 2, tp, srows, d_model), BF16),
            pltpu.VMEM((rows, d_model), BF16),
            pltpu.VMEM((2, rows, ep * cap), BF16),
            pltpu.VMEM((ep, cap, rows), BF16),
            pltpu.VMEM((ep, cap, rows), BF16),
            pltpu.VMEM((ep, rows, d_model), BF16),
            pltpu.VMEM((ep, cap, d_model), BF16),
            pltpu.VMEM((ep * cap, tp * own_rows), BF16),
            pltpu.VMEM((ep, cap, d_model), BF16),
            pltpu.VMEM((ep, cap, d_model), BF16),
            dma((moves, near)),
            dma((moves, tp)),
            dma((moves, 2, far, far)),
            dma((moves, 2, tp)),
            dma((3,)),
            dma((3,)),
            dma((ep,)),
            dma((ep,)),
            dma((2, ep // 2)),
            dma((ep // 2,)),
            dma((ep // 2,)),
            dma((ep // 2,)),
            dma((CHUNKS, ep)),
            dma((CHUNKS, ep)),
        ],
        compiler_params=pltpu.CompilerParams(
            collective_id=0, has_side_effects=True, vmem_limit_bytes=62 * 1024 * 1024
        ),
        name="moe",
    )(tokens, norm_gain.reshape(1, d_model), expert_ids, gate_weights, eg[0], eu[0], ed[0], sg, su, sd)


def solution(mesh):
    in_specs = (
        P(("ep", "tp"), None),
        P(),
        P(("ep", "tp"), None),
        P(("ep", "tp"), None),
        P("ep", "tp", None),
        P("ep", "tp", None),
        P("ep", "tp", None),
        P("tp", None),
        P("tp", None),
        P("tp", None),
    )
    out_specs = P(("ep", "tp"), None)
    return jax.shard_map(
        functools.partial(body, mesh.shape["ep"], mesh.shape["tp"]),
        mesh=mesh, in_specs=in_specs, out_specs=out_specs, check_vma=False,
    )
```

time: 112 us -> 106 us (0.946)
  the two profiles are of different devices: /device:TPU:9 before, /device:TPU:0 now
where the time goes in v2:
time: 106 us
  Pallas kernels  102 us (96%)
  local copies, waits for them, and re-layouts  4.03 us (4%)
    pallas_call x1, Pallas kernels, body(): pl.pallas_call(functools.partial(kernel, ep, tp, xs, ys, cap), out_shape=...  102 us
    unnamed x7, local copies, waits for them, and re-layouts  4.03 us

profile of v2, /device:TPU:0, one launch (start us, length us, event | category | flops | bytes accessed | tf_op | source)
XLA Modules:
  0.0 106.3 jit_solution(10311236144144494670)
XLA Ops:
  0.0 0.0 copy-start
  0.0 0.7 copy-done
  0.7 0.0 copy-start.1
  0.7 0.7 copy.11.ids_ref
  1.4 0.0 copy-done.1
  1.4 0.7 copy.12.gw_ref
  2.2 102.3 %moe.1 = bf16[128,2048]{1,0:T(8,128)(2,1)} custom-call(bf16[128,2048]{1,0:T(8,128)(2,1)} %tok_ref.1, f32[1,2048]{1,0:T(1,128)} %bitcast.7, s32[128,2]{1,0:T(8,128)} %copy.11.ids_ref, f32[128,2]{1,0:T(8,128)} %copy.12.gw_ref, bf16[128,2048]{1,0:T(8,128)(2,1)} %bitcast.4, bf16[128,2048]{1,0:T(8,128)(2,1)} %bitcast.5, bf16[128,2048]{1,0:T(8,128)(2,1)} %bitcast.6, ...), custom_call_target="tpu_custom_call" | custom-call | tf_op jit(solution)/shard_map/moe/pallas_call | solution.py:333
  104.4 1.9 %copy.14 = bf16[128,2048]{1,0:T(8,128)(2,1)} copy(bf16[128,2048]{1,0:T(8,128)(2,1)} %moe.1) | data formatting | bytes 1048576
Async XLA Ops:
  0.0 0.7 copy-start
  0.7 0.7 copy-start.1

commit v3 on v2

--- a/solution.py
+++ b/solution.py
@@ -24,7 +24,7 @@
 
 def kernel(
     ep, tp, xs, ys, cap,
-    tok_ref, gain_ref, ids_ref, gw_ref, eg, eu, ed, sg, su, sd, out_ref,
+    tok_ref, gain_ref, route_ref, eg, eu, ed, sg, su, sd, out_ref,
     wts, swts, normed, mix, spread, pick, tokens, arrived, hidden, results, returned,
     s1, r1, s2, r2, s3, r3, sp, rp, st, rt, sd2, rd2, sb, rb,
 ):
@@ -47,7 +47,11 @@
     row_peers = [at(0, i) for i in range(1, xs)]
     col_peers = [at(i, 0) for i in range(1, ys)]
     diagonal = [at(i, j) for i in range(1, ys) for j in range(1, xs)]
-    ep_peers = [lax.rem(e + i, ep) for i in range(1, ep)]
+    if ep & (ep - 1) == 0:
+        bits = [1 << b for b in range(ep.bit_length() - 1)]
+        ep_peers = [sum((e // b + i // b) % 2 * b for b in bits) for i in range(ep - 1, 0, -1)]
+    else:
+        ep_peers = [lax.rem(e + i, ep) for i in range(1, ep)]
 
     barrier = pltpu.get_barrier_semaphore()
     for p in row_peers + col_peers:
@@ -138,9 +142,9 @@
     over(z, tok_ref).start()
     first(1)
 
-    ids = ids_ref[...]
-    chosen = ids.shape[1]
-    labels = lax.broadcasted_iota(jnp.int32, (rows, ep), 1)
+    chosen = route_ref.shape[1] // 2
+    ids = route_ref[:, :chosen]
+    labels = lax.broadcasted_iota(jnp.int32, (rows, ep), 1).astype(F32)
     one_hot = [(ids[:, k : k + 1] == labels).astype(F32) for k in range(chosen)]
     hits = sum(one_hot[1:], one_hot[0])
     lower = (
@@ -151,10 +155,10 @@
     weights = jnp.zeros((rows, slots), F32)
     placing = jnp.zeros((rows, slots), F32)
     for k in range(chosen):
-        place = ids[:, k : k + 1].astype(F32) * cap + jnp.sum(before * one_hot[k], axis=1, keepdims=True)
+        place = ids[:, k : k + 1] * cap + jnp.sum(before * one_hot[k], axis=1, keepdims=True)
         hit = (place == slot_ids).astype(F32)
         placing = placing + hit
-        weights = weights + gw_ref[:, k : k + 1] * hit
+        weights = weights + route_ref[:, chosen + k : chosen + k + 1] * hit
     spread[...] = placing.T.astype(BF16).reshape(ep, cap, rows)
     high = weights.astype(BF16)
     mix[0] = high
@@ -213,15 +217,17 @@
             first_done(1)
             second(1)
             first(2)
-            first(3)
         else:
             packs(step)
     if nz == 1:
         first_done(1)
         second(1)
         first(2)
-        first(3)
-
+
+    first_done(2)
+    second(2)
+    first(3)
+    first(4)
     second_done(0)
     second_done(1)
     per = max(1, min(tp, 256 // own_rows))
@@ -238,16 +244,7 @@
 
     total = last + 3
     for n in range(CHUNKS):
-        a = n + 2
-        if n == 0:
-            first_done(a)
-            second(a)
-            first(a + 2)
-        first_done(a + 1)
-        second(a + 1)
-        if a + 3 < total:
-            first(a + 3)
-        second_done(a)
+        second_done(n + 2)
         cols = slice(n * piece, (n + 1) * piece)
         down = wts[2, :, :, cols].reshape(tp * own_rows, piece)
         o = jnp.dot(hidden[...], down, preferred_element_type=F32).astype(BF16)
@@ -257,14 +254,18 @@
             c.start()
             sends.append(c)
         returned[e, :, cols] = results[e, :, cols]
+        first_done(n + 3)
+        second(n + 3)
+        if n + 5 < total:
+            first(n + 5)
 
     def swap(a):
         return remote(swts.at[a, core], swts.at[a, core], s3.at[a], r3.at[a], {"ep": partner})
 
+    for a in range(1, 3):
+        first_done(last + a)
+        second(last + a)
     for a in range(3):
-        if a > 0:
-            first_done(last + a)
-            second(last + a)
         second_done(last + a)
         c = swap(a)
         c.start()
@@ -326,6 +327,7 @@
     own_rows = eg.shape[1]
     srows = sg.shape[0] // 2
     near = xs + ys - 2
+    route = jnp.concatenate([expert_ids.astype(F32), gate_weights], axis=1)
     far = max(xs, ys)
     moves = 2 + CHUNKS + 3
     dma = pltpu.SemaphoreType.DMA
@@ -333,7 +335,7 @@
     return pl.pallas_call(
         functools.partial(kernel, ep, tp, xs, ys, cap),
         out_shape=jax.ShapeDtypeStruct((rows, d_model), BF16),
-        in_specs=[vm] * 10,
+        in_specs=[vm] * 9,
         out_specs=vm,
         scratch_shapes=[
             pltpu.VMEM((3, tp, own_rows, d_model), BF16),
@@ -366,7 +368,7 @@
             collective_id=0, has_side_effects=True, vmem_limit_bytes=62 * 1024 * 1024
         ),
         name="moe",
-    )(tokens, norm_gain.reshape(1, d_model), expert_ids, gate_weights, eg[0], eu[0], ed[0], sg, su, sd)
+    )(tokens, norm_gain.reshape(1, d_model), route, eg[0], eu[0], ed[0], sg, su, sd)
 
 
 def solution(mesh):

time: 106 us -> 104 us (0.981)
  Pallas kernels: 102 us -> 100 us
    pallas_call x1, Pallas kernels: 102 us -> 100 us  [body(): pl.pallas_call(functools.partial(kernel, ep, tp, xs, ys, cap), out_shape=...]
    unnamed x7 -> x5, local copies, waits for them, and re-layouts: 4.03 us -> 3.24 us
where the time goes in v3:
time: 104 us
  Pallas kernels  100 us (96%)
  local copies, waits for them, and re-layouts  3.98 us (4%)
    pallas_call x1, Pallas kernels, body(): pl.pallas_call(functools.partial(kernel, ep, tp, xs, ys, cap), out_shape=...  100 us
    unnamed x5, local copies, waits for them, and re-layouts  3.24 us

profile of v3, /device:TPU:0, one launch (start us, length us, event | category | flops | bytes accessed | tf_op | source)
XLA Modules:
  0.0 104.0 jit_solution(434288114910615915)
XLA Ops:
  0.0 0.0 copy-start
  0.0 0.7 copy-done
  0.7 0.0 copy-start.1
  0.7 0.7 copy-done.1
  1.4 0.7 copy.13.route_ref
  2.1 100.0 %moe.1 = bf16[128,2048]{1,0:T(8,128)(2,1)} custom-call(bf16[128,2048]{1,0:T(8,128)(2,1)} %tok_ref.1, f32[1,2048]{1,0:T(1,128)} %bitcast.7, f32[128,4]{1,0:T(8,128)} %copy.13.route_ref, bf16[128,2048]{1,0:T(8,128)(2,1)} %bitcast.4, bf16[128,2048]{1,0:T(8,128)(2,1)} %bitcast.5, bf16[128,2048]{1,0:T(8,128)(2,1)} %bitcast.6, bf16[128,2048]{1,0:T(8,128)(2,1)} %sg.1, ...), custom_call_target="tpu_custom_call" | custom-call | tf_op jit(solution)/shard_map/moe/pallas_call | solution.py:335
  102.1 1.9 %copy.15 = bf16[128,2048]{1,0:T(8,128)(2,1)} copy(bf16[128,2048]{1,0:T(8,128)(2,1)} %moe.1) | data formatting | bytes 1048576
  (2 shorter events, 0.0 us)
Async XLA Ops:
  0.0 0.7 copy-start
  0.7 0.7 copy-start.1
